TPU v7x, 32 devices: a whole 2x2x4 slice. The times are simulated.
32 devices in a mesh: gr: 2 (over x), sp: 4 (over z), tp: 4 (over y, core).
Axes of the slice: x: 2, y: 2, z: 4, core: 2. Of those that a mesh axis runs over, the one named last changes fastest.
Arguments:
- tokens: bfloat16 [8, 8192, 2048], P('gr', ('sp', 'tp')), parts along dimension 0, may hold values from -6 to 6
- norm_gain: float32 [2048], replicated, may hold values from 0.1 to 1.9
- w_key: bfloat16 [2048, 256], replicated, may hold values from -0.125 to 0.125
- w_value: bfloat16 [2048, 256], replicated, may hold values from -0.125 to 0.125
- new_query: bfloat16 [8, 32, 64], P('gr'), parts along dimension 0, may hold values from -360 to 360
- cum_gate: float32 [8, 4, 8192], P(('gr', 'sp'), 'tp'), parts along dimension 0, may hold values from -1025 to 0, as said below
Outputs:
- kv_cache: bfloat16 [8, 4, 8192, 128], P(('gr', 'sp'), 'tp'), parts along dimension 0
- first_read: float32 [8, 32, 64], P('gr'), parts along dimension 0
There are 2 independent parts, one for each index of `gr`. A program takes and returns all parts, laid end to end along the dimension named above; an argument that names none is the same for every part. Nothing has to cross between parts.
Inputs may be any that keep to these rules, and one draw needn't show every extreme that they name: `cum_gate`: for each sequence and key head, the running sum along the positions of the sequence of negative log forget gates; it never rises from one position to the next.
All inputs are finite; a program needn't handle non-finite values.
Results may differ from a plain program's by a relative error of at most 0.0014.
The roundings to bfloat16 on the way count: a program that leaves them out, or rounds other values in their place, can miss the bound.
Values may be sent and summed in bfloat16 or wider, within the bound.
A program may use at most 64 MiB of HBM per device.

v0:
```python
import functools

import jax
import jax.numpy as jnp
from jax import lax
from jax.experimental import pallas as pl
from jax.experimental.pallas import tpu as pltpu
from jax.sharding import PartitionSpec as P

HD = 64
NORM_FLOOR = 0.05
SCORE_FLOOR = -1e30
MESH = pl.DeviceIdType.MESH
TILE = 256
CHUNKS = 4
NORM_ROWS = 16
VMEM_BYTES = 60_000_000


def sequence_at(step, own, count):
    low = own < count // 2
    first = jnp.where(low, count - 1 - step, step)
    following = jnp.where(low, count - 2 - step, step + 1)
    own_step = jnp.where(low, count - 1 - own, own)
    shifted = jnp.where(step >= own_step, following, first)
    return jnp.where(step == count - 1, own, shifted)


def kernel(
    sizes,
    tokens_hbm,
    gain_hbm,
    wk_hbm,
    wv_hbm,
    query_hbm,
    gate_hbm,
    cache_ref,
    read_ref,
    tok_buf,
    wk_buf,
    wv_buf,
    gain_ref,
    query_ref,
    gate_ref,
    norm_buf,
    staging,
    gates_in,
    own_parts,
    parts_in,
    partials,
    tok_sem,
    w_sem,
    send_sem,
    recv_sem,
    part_send_sem,
    part_recv_sem,
    gate_send_sem,
    gate_recv_sem,
    early_send_sem,
    early_recv_sem,
    own_sem,
):
    sp_count, tp_count, seqs, heads, positions, width = sizes
    devices = sp_count * tp_count
    classes, halves = sp_count // seqs, tp_count // heads
    piece = positions // (classes * halves)
    sp, tp = lax.axis_index("sp"), lax.axis_index("tp")
    me = sp * tp_count + tp
    seq_me, head_me = sp // classes, tp // halves
    tile = min(TILE, positions)
    tiles = positions // tile
    sub = min(piece, tile)

    def token_copy(step, part):
        seq = sequence_at(step, seq_me, seqs)
        rows = pl.ds(part * tile, tile)
        return pltpu.make_async_copy(
            tokens_hbm.at[seq, rows, :], tok_buf.at[step, rows, :], tok_sem.at[step, part]
        )

    k_copy = pltpu.make_async_copy(wk_hbm, wk_buf, w_sem.at[0])
    v_copy = pltpu.make_async_copy(wv_hbm, wv_buf, w_sem.at[1])
    gain_copy = pltpu.make_async_copy(gain_hbm, gain_ref, w_sem.at[2])
    query_copy = pltpu.make_async_copy(query_hbm, query_ref, w_sem.at[3])
    gate_copy = pltpu.make_async_copy(gate_hbm, gate_ref, w_sem.at[4])
    gain_copy.start()
    gate_copy.start()
    query_copy.start()
    token_copy(0, 0).start()
    k_copy.start()
    v_copy.start()
    for step in range(seqs):
        for part in range(tiles):
            if step or part:
                token_copy(step, part).start()
    gain_copy.wait()

    barrier = pltpu.get_barrier_semaphore()

    def greet(other, carry):
        @pl.when(other != me)
        def _():
            pl.semaphore_signal(
                barrier,
                inc=1,
                device_id={"sp": other // tp_count, "tp": other % tp_count},
                device_id_type=MESH,
            )

        return carry

    lax.fori_loop(0, devices, greet, 0)

    def project(index, carry):
        step, part = index // tiles, index % tiles
        seq = sequence_at(step, seq_me, seqs)
        row0 = pl.multiple_of(part * tile, tile)
        token_copy(step, part).wait()
        gain = gain_ref[...]
        for piece_row in range(0, tile, NORM_ROWS):
            block = tok_buf[step, pl.ds(row0 + piece_row, NORM_ROWS), :].astype(jnp.float32)
            mean = jnp.mean(block * block, axis=-1, keepdims=True)
            normed = block * lax.rsqrt(mean + NORM_FLOOR) * gain
            norm_buf[pl.ds(piece_row, NORM_ROWS), :] = normed.astype(jnp.bfloat16)

        @pl.when(index == 0)
        def _():
            k_copy.wait()
            v_copy.wait()

        normed_tile = norm_buf[...]
        keys = jnp.dot(normed_tile, wk_buf[...], preferred_element_type=jnp.float32)
        values = jnp.dot(normed_tile, wv_buf[...], preferred_element_type=jnp.float32)
        keys = keys.astype(jnp.bfloat16)
        values = values.astype(jnp.bfloat16)
        for head in range(heads):
            cols = slice(head * HD, (head + 1) * HD)
            both = jnp.concatenate([keys[:, cols], values[:, cols]], axis=1)
            staging[seq * heads + head, pl.ds(row0, tile), :] = both

        @pl.when(index == 0)
        def _():
            pl.semaphore_wait(barrier, devices - 1)
            gate_copy.wait()
            for_others(send_gate)

        @pl.when(step == 0)
        def _():
            send_tile(index)

        return carry

    window = max(piece, 128)

    def for_others(body):
        def visit(other, carry):
            @pl.when(other != me)
            def _():
                body(other)

            return carry

        lax.fori_loop(0, devices, visit, 0)

    def place(other):
        return {"sp": other // tp_count, "tp": other % tp_count}

    def gate_window(other):
        start = pl.multiple_of(other * piece // window * window, window)
        return gate_ref.at[:, pl.ds(start, window)]

    def send_gate(other):
        pltpu.make_async_remote_copy(
            src_ref=gate_window(other),
            dst_ref=gates_in.at[me],
            send_sem=gate_send_sem,
            recv_sem=gate_recv_sem,
            device_id=place(other),
            device_id_type=MESH,
        ).start()

    def send_tile(index):
        step, part = index // tiles, index % tiles
        seq = sequence_at(step, seq_me, seqs)
        row0 = part * tile
        for head in range(heads):
            for piece_row in range(0, tile, sub):
                row = pl.multiple_of(row0 + piece_row, sub)
                slot = row // piece
                to_sp = seq * classes + slot // halves
                to_tp = head * halves + slot % halves
                dest = to_sp * tp_count + to_tp
                landing = pl.multiple_of(me * piece + row % piece, sub)
                source = staging.at[seq * heads + head, pl.ds(row, sub), :]
                target = cache_ref.at[pl.ds(landing, sub), :]

                @pl.when(dest != me)
                def _():
                    pltpu.make_async_remote_copy(
                        src_ref=source,
                        dst_ref=target,
                        send_sem=send_sem,
                        recv_sem=recv_sem,
                        device_id={"sp": to_sp, "tp": to_tp},
                        device_id_type=MESH,
                    ).start()

                @pl.when(dest == me)
                def _():
                    pltpu.make_async_copy(source, target, own_sem).start()

    def send_tiles(first, last):
        def visit(index, carry):
            send_tile(index)
            return carry

        lax.fori_loop(first, last, visit, 0)

    def wait_bytes(ref, sem):
        pltpu.make_async_copy(ref, ref, sem).wait()

    lax.fori_loop(0, seqs * tiles, project, 0)

    query_copy.wait()
    group = query_ref.shape[2]
    others = parts_in.at[pl.ds(0, devices - 1)]
    gates_in[me] = gate_ref[:, pl.ds(pl.multiple_of(me * piece // window * window, window), window)]
    other_gates = gates_in.at[pl.ds(0, devices - 1)]
    wait_bytes(other_gates, gate_recv_sem)
    lane = lax.broadcasted_iota(jnp.int32, (group, 2 * HD), 1)
    line = lax.broadcasted_iota(jnp.int32, (group, 2 * HD), 0)
    half = group // 2

    def pack(ref, slot, top, total, out):
        folded = jnp.concatenate([out[:half], out[half:]], axis=1)
        stats = jnp.where(lane == line, top, 0.0) + jnp.where(lane == line + group, total, 0.0)
        for k in range(half):
            ref[slot, :, k * 2 * HD : (k + 1) * 2 * HD] = folded[k : k + 1]
        ref[slot, :, half * 2 * HD :] = jnp.sum(stats, axis=0, keepdims=True)

    def unpack(ref, slot):
        rows = [ref[slot, :, k * 2 * HD : (k + 1) * 2 * HD] for k in range(half + 1)]
        out = jnp.concatenate([r[:, :HD] for r in rows[:half]] + [r[:, HD:] for r in rows[:half]])
        top = jnp.sum(jnp.where(lane == line, rows[half], 0.0), axis=1, keepdims=True)
        total = jnp.sum(jnp.where(lane == line + group, rows[half], 0.0), axis=1, keepdims=True)
        return top, total, out

    def merge(left, right):
        best = jnp.maximum(left[0], right[0])
        scale_left, scale_right = jnp.exp(left[0] - best), jnp.exp(right[0] - best)
        total = left[1] * scale_left + right[1] * scale_right
        return best, total, left[2] * scale_left + right[2] * scale_right

    def attend(seq, carry):
        for head in range(heads):
            query = query_ref[seq, head]
            query = jnp.concatenate([query, jnp.zeros_like(query)], axis=1)
            for slot in range(classes * halves):
                dest = (seq * classes + slot // halves) * tp_count + head * halves + slot % halves
                block = staging[seq * heads + head, slot * piece : (slot + 1) * piece, :]
                gates = gates_in[dest]
                choices = [gates[:, k * piece : (k + 1) * piece] for k in range(window // piece)]
                gate = choices[0]
                for k in range(1, len(choices)):
                    gate = jnp.where(me % (window // piece) == k, choices[k], gate)
                scores = lax.dot_general(
                    query, block, (((1,), (1,)), ((), ())), preferred_element_type=jnp.float32
                )
                scores = scores * HD ** (-0.5) - gate
                top = jnp.max(scores, axis=1, keepdims=True)
                weights = jnp.exp(scores - top)
                total = jnp.sum(weights, axis=1, keepdims=True)
                first = weights.astype(jnp.bfloat16)
                rest = weights - first.astype(jnp.float32)
                second = rest.astype(jnp.bfloat16)
                third = (rest - second.astype(jnp.float32)).astype(jnp.bfloat16)
                summed = jnp.dot(first, block, preferred_element_type=jnp.float32)
                summed += jnp.dot(second, block, preferred_element_type=jnp.float32)
                summed += jnp.dot(third, block, preferred_element_type=jnp.float32)
                pack(own_parts, dest, top, total, summed[:, HD:])
        return carry

    lax.fori_loop(0, seqs, attend, 0)
    parts_in[me] = own_parts[me]

    def send_part(other):
        pltpu.make_async_remote_copy(
            src_ref=own_parts.at[other],
            dst_ref=parts_in.at[me],
            send_sem=early_send_sem,
            recv_sem=early_recv_sem,
            device_id=place(other),
            device_id_type=MESH,
        ).start()

    for_others(send_part)
    held = tiles + max(tiles // 2, 1)
    send_tiles(2 * tiles, seqs * tiles)
    send_tiles(tiles, held)

    wait_bytes(others, early_recv_sem)
    merged = lax.fori_loop(
        1, devices, lambda n, held_sum: merge(held_sum, unpack(parts_in, n)), unpack(parts_in, 0)
    )
    pack(partials, me, *merged)

    def send_read(other):
        pltpu.make_async_remote_copy(
            src_ref=partials.at[me],
            dst_ref=partials.at[me],
            send_sem=part_send_sem,
            recv_sem=part_recv_sem,
            device_id=place(other),
            device_id_type=MESH,
        ).start()

    for_others(send_read)
    send_tiles(held, 2 * tiles)

    wait_bytes(partials.at[pl.ds(0, devices - 1)], part_recv_sem)
    for seq in range(seqs):
        for head in range(heads):
            slots = [
                unpack(partials, (seq * classes + c) * tp_count + head * halves + b)
                for c in range(classes)
                for b in range(halves)
            ]
            _, total, out = functools.reduce(merge, slots)
            read_ref[seq, pl.ds(head * group, group), :] = out / total
    wait_bytes(other_gates, gate_send_sem)
    wait_bytes(others, early_send_sem)
    wait_bytes(others, part_send_sem)
    wait_bytes(cache_ref.at[pl.ds(0, piece), :], own_sem)
    sent = cache_ref.at[pl.ds(0, (devices - 1) * piece), :]
    wait_bytes(sent, send_sem)
    wait_bytes(sent, recv_sem)


def settle(cache_in, read_in, cache_out, read_out, cache_buf, read_buf, sems):
    chunks = sems.shape[1] - 1
    rows = cache_in.shape[0] // chunks
    ins, outs = [], []
    for k in range(chunks):
        part = pl.ds(k * rows, rows)
        ins.append(pltpu.make_async_copy(cache_in.at[part], cache_buf.at[part], sems.at[0, k]))
        outs.append(pltpu.make_async_copy(cache_buf.at[part], cache_out.at[part], sems.at[1, k]))
    ins.append(pltpu.make_async_copy(read_in, read_buf, sems.at[0, chunks]))
    outs.append(pltpu.make_async_copy(read_buf, read_out, sems.at[1, chunks]))
    for copy in ins:
        copy.start()
    for copy_in, copy_out in zip(ins, outs):
        copy_in.wait()
        copy_out.start()
    for copy in outs:
        copy.wait()


def solution(mesh):
    sp_count, tp_count = mesh.shape["sp"], mesh.shape["tp"]
    devices = sp_count * tp_count

    def shards(tokens, norm_gain, w_key, w_value, new_query, cum_gate):
        seqs, positions, width = tokens.shape
        heads = w_key.shape[1] // HD
        columns = w_key.shape[1]
        query_heads = new_query.shape[1]
        group = query_heads // heads
        length = cum_gate.shape[-1]
        tile = min(TILE, positions)
        sizes = (sp_count, tp_count, seqs, heads, positions, width)
        vmem = pl.BlockSpec(memory_space=pltpu.VMEM)
        anywhere = pl.BlockSpec(memory_space=pltpu.HBM)
        cache, first_read = pl.pallas_call(
            functools.partial(kernel, sizes),
            out_shape=(
                jax.ShapeDtypeStruct((length, 2 * HD), jnp.bfloat16),
                jax.ShapeDtypeStruct((seqs, query_heads, HD), jnp.float32),
            ),
            in_specs=[anywhere] * 6,
            out_specs=(anywhere, vmem),
            scratch_shapes=[
                pltpu.VMEM((seqs, positions, width), jnp.bfloat16),
                pltpu.VMEM((width, columns), jnp.bfloat16),
                pltpu.VMEM((width, columns), jnp.bfloat16),
                pltpu.VMEM((1, width), jnp.float32),
                pltpu.VMEM((seqs, heads, group, HD), jnp.bfloat16),
                pltpu.VMEM((1, length), jnp.float32),
                pltpu.VMEM((tile, width), jnp.bfloat16),
                pltpu.VMEM((seqs * heads, positions, 2 * HD), jnp.bfloat16),
                pltpu.VMEM((devices, 1, max(length // devices, 128)), jnp.float32),
                pltpu.VMEM((devices, 1, (group // 2 + 1) * 2 * HD), jnp.float32),
                pltpu.VMEM((devices, 1, (group // 2 + 1) * 2 * HD), jnp.float32),
                pltpu.VMEM((devices, 1, (group // 2 + 1) * 2 * HD), jnp.float32),
                pltpu.SemaphoreType.DMA((seqs, positions // tile)),
                pltpu.SemaphoreType.DMA((5,)),
                *[pltpu.SemaphoreType.DMA] * 9,
            ],
            compiler_params=pltpu.CompilerParams(
                collective_id=0, has_side_effects=True, vmem_limit_bytes=VMEM_BYTES
            ),
        )(
            tokens,
            norm_gain.reshape(1, width),
            w_key,
            w_value,
            new_query.reshape(seqs, heads, group, HD),
            cum_gate.reshape(1, length),
        )
        cache, first_read = pl.pallas_call(
            settle,
            out_shape=(
                jax.ShapeDtypeStruct(cache.shape, cache.dtype),
                jax.ShapeDtypeStruct(first_read.shape, first_read.dtype),
            ),
            in_specs=[anywhere] * 2,
            out_specs=(anywhere, anywhere),
            scratch_shapes=[
                pltpu.VMEM(cache.shape, cache.dtype),
                pltpu.VMEM(first_read.shape, first_read.dtype),
                pltpu.SemaphoreType.DMA((2, CHUNKS + 1)),
            ],
            compiler_params=pltpu.CompilerParams(vmem_limit_bytes=VMEM_BYTES),
        )(cache, first_read)
        return cache.reshape(1, 1, length, 2 * HD), first_read

    in_specs = (
        P("gr", ("sp", "tp"), None),
        P(),
        P(),
        P(),
        P("gr", None, None),
        P(("gr", "sp"), "tp", None),
    )
    out_specs = (P(("gr", "sp"), "tp", None, None), P("gr", None, None))
    return jax.shard_map(shards, mesh=mesh, in_specs=in_specs, out_specs=out_specs, check_vma=False)
```

profile of v0, /device:TPU:13, one launch (start us, length us, event | category | flops | bytes accessed | tf_op | source)
XLA Modules:
  0.0 58.5 jit_solution(4361422344092351852)
XLA Ops:
  0.6 55.4 %shard_map.77 = (bf16[8192,128]{1,0:T(8,128)(2,1)}, f32[4,32,64]{2,1,0:T(8,128)}) custom-call(bf16[4,512,2048]{2,1,0:T(8,128)(2,1)} %tokens_hbm.1, f32[1,2048]{1,0:T(1,128)} %bitcast.6, bf16[2048,256]{1,0:T(8,128)(2,1)} %wk_hbm.1, bf16[2048,256]{1,0:T(8,128)(2,1)} %wv_hbm.1, bf16[4,4,8,64]{3,2,1,0:T(8,128)(2,1)} %bitcast.4, f32[1,8192]{1,0:T(1,128)} %bitcast.5), custom_call_target="tpu_custom_call" | custom-call | tf_op jit(solution)/shard_map/pallas_call | solution.py:373
  56.1 2.4 %shard_map.78 = (bf16[8192,128]{1,0:T(8,128)(2,1)}, f32[4,32,64]{2,1,0:T(8,128)}) custom-call(bf16[8192,128]{1,0:T(8,128)(2,1)} %get-tuple-element.6.cache_in, f32[4,32,64]{2,1,0:T(8,128)} %get-tuple-element.7.read_in), custom_call_target="tpu_custom_call" | custom-call | tf_op jit(solution)/shard_map/pallas_call | solution.py:409
where the time goes:
time: 58.7 us; the launch traced here: 58.5 us
  Pallas kernels  57.9 us (99%)
  between operations  0.64 us (1%)
    pallas_call x1, Pallas kernels, shards(): pl.pallas_call(functools.partial(kernel, sizes), out_shape=(jax.ShapeDtyp...  55.4 us
    pallas_call x1, Pallas kernels, shards(): pl.pallas_call(settle, out_shape=(jax.ShapeDtypeStruct(cache.shape, cache...  2.45 us

commit v1 on v0

--- a/solution.py
+++ b/solution.py
@@ -336,22 +336,14 @@
     wait_bytes(sent, recv_sem)
 
 
-def settle(cache_in, read_in, cache_out, read_out, cache_buf, read_buf, sems):
-    chunks = sems.shape[1] - 1
-    rows = cache_in.shape[0] // chunks
-    ins, outs = [], []
-    for k in range(chunks):
-        part = pl.ds(k * rows, rows)
-        ins.append(pltpu.make_async_copy(cache_in.at[part], cache_buf.at[part], sems.at[0, k]))
-        outs.append(pltpu.make_async_copy(cache_buf.at[part], cache_out.at[part], sems.at[1, k]))
-    ins.append(pltpu.make_async_copy(read_in, read_buf, sems.at[0, chunks]))
-    outs.append(pltpu.make_async_copy(read_buf, read_out, sems.at[1, chunks]))
-    for copy in ins:
+def settle(cache_in, read_in, cache_out, read_out, sems):
+    copies = [
+        pltpu.make_async_copy(cache_in, cache_out, sems.at[0]),
+        pltpu.make_async_copy(read_in, read_out, sems.at[1]),
+    ]
+    for copy in copies:
         copy.start()
-    for copy_in, copy_out in zip(ins, outs):
-        copy_in.wait()
-        copy_out.start()
-    for copy in outs:
+    for copy in copies:
         copy.wait()
 
 
@@ -373,11 +365,11 @@
         cache, first_read = pl.pallas_call(
             functools.partial(kernel, sizes),
             out_shape=(
-                jax.ShapeDtypeStruct((length, 2 * HD), jnp.bfloat16),
-                jax.ShapeDtypeStruct((seqs, query_heads, HD), jnp.float32),
+                pltpu.VMEM((length, 2 * HD), jnp.bfloat16),
+                pltpu.VMEM((seqs, query_heads, HD), jnp.float32),
             ),
             in_specs=[anywhere] * 6,
-            out_specs=(anywhere, vmem),
+            out_specs=(vmem, vmem),
             scratch_shapes=[
                 pltpu.VMEM((seqs, positions, width), jnp.bfloat16),
                 pltpu.VMEM((width, columns), jnp.bfloat16),
@@ -412,15 +404,14 @@
                 jax.ShapeDtypeStruct(cache.shape, cache.dtype),
                 jax.ShapeDtypeStruct(first_read.shape, first_read.dtype),
             ),
-            in_specs=[anywhere] * 2,
+            in_specs=[vmem] * 2,
             out_specs=(anywhere, anywhere),
-            scratch_shapes=[
-                pltpu.VMEM(cache.shape, cache.dtype),
-                pltpu.VMEM(first_read.shape, first_read.dtype),
-                pltpu.SemaphoreType.DMA((2, CHUNKS + 1)),
-            ],
+            scratch_shapes=[pltpu.SemaphoreType.DMA((2,))],
             compiler_params=pltpu.CompilerParams(vmem_limit_bytes=VMEM_BYTES),
-        )(cache, first_read)
+        )(
+            pltpu.with_memory_space_constraint(cache, pltpu.VMEM),
+            pltpu.with_memory_space_constraint(first_read, pltpu.VMEM),
+        )
         return cache.reshape(1, 1, length, 2 * HD), first_read
 
     in_specs = (

time: 58.7 us -> 57.2 us (0.974)
  Pallas kernels: 57.9 us -> 56 us
    pallas_call x1, Pallas kernels: 2.45 us -> 1.34 us  [shards(): pl.pallas_call(settle, out_shape=(jax.ShapeDtypeStruct(cache.shape, cache...]
    pallas_call x1, Pallas kernels: 55.4 us -> 54.7 us  [shards(): pl.pallas_call(functools.partial(kernel, sizes), out_shape=(pltpu.VMEM((l...]
where the time goes in v1:
time: 57.2 us; the launch traced here: 56.7 us
  Pallas kernels  56 us (98%)
  between operations  0.64 us (1%)
    pallas_call x1, Pallas kernels, shards(): pl.pallas_call(functools.partial(kernel, sizes), out_shape=(pltpu.VMEM((l...  54.7 us
    pallas_call x1, Pallas kernels, shards(): pl.pallas_call(settle, out_shape=(jax.ShapeDtypeStruct(cache.shape, cache...  1.34 us

profile of v1, /device:TPU:13, one launch (start us, length us, event | category | flops | bytes accessed | tf_op | source)
XLA Modules:
  0.0 56.7 jit_solution(635654097125319879)
XLA Ops:
  0.6 54.7 %shard_map.77 = (bf16[8192,128]{1,0:T(8,128)(2,1)S(1)}, f32[4,32,64]{2,1,0:T(8,128)S(1)}) custom-call(bf16[4,512,2048]{2,1,0:T(8,128)(2,1)} %tokens_hbm.1, f32[1,2048]{1,0:T(1,128)} %bitcast.6, bf16[2048,256]{1,0:T(8,128)(2,1)} %wk_hbm.1, bf16[2048,256]{1,0:T(8,128)(2,1)} %wv_hbm.1, bf16[4,4,8,64]{3,2,1,0:T(8,128)(2,1)} %bitcast.4, f32[1,8192]{1,0:T(1,128)} %bitcast.5), custom_call_target="tpu_custom_call" | custom-call | tf_op jit(solution)/shard_map/pallas_call | solution.py:365
  55.3 1.3 %shard_map.78 = (bf16[8192,128]{1,0:T(8,128)(2,1)}, f32[4,32,64]{2,1,0:T(8,128)}) custom-call(bf16[8192,128]{1,0:T(8,128)(2,1)S(1)} %get-tuple-element.6.cache_in, f32[4,32,64]{2,1,0:T(8,128)S(1)} %get-tuple-element.7.read_in), custom_call_target="tpu_custom_call" | custom-call | tf_op jit(solution)/shard_map/pallas_call | solution.py:401

commit v2 on v1

v2 whole, which is shorter than its diff:
```python
import functools

import jax
import jax.numpy as jnp
from jax import lax
from jax.experimental import pallas as pl
from jax.experimental.pallas import tpu as pltpu
from jax.sharding import PartitionSpec as P

HD = 64
NORM_FLOOR = 0.05
SCORE_FLOOR = -1e30
MESH = pl.DeviceIdType.MESH
TILE = 256
NORM_ROWS = 16
VMEM_BYTES = 60_000_000


def is_edge(own, count):
    return (own == 0) | (own == count - 1)


def sequence_at(step, own, count):
    low = own < count // 2
    moved = jnp.where(step == 0, count - 2, jnp.where(step <= count - 2, step - 1, step))
    turn = jnp.where(is_edge(own, count), moved, step)
    first = jnp.where(low, count - 1 - turn, turn)
    following = jnp.where(low, count - 2 - turn, turn + 1)
    own_step = jnp.where(low, count - 1 - own, own)
    shifted = jnp.where(turn >= own_step, following, first)
    return jnp.where(step == count - 1, own, shifted)


def kernel(
    sizes,
    tokens_hbm,
    gain_hbm,
    wk_hbm,
    wv_hbm,
    query_hbm,
    gate_hbm,
    cache_ref,
    read_ref,
    tok_buf,
    wk_buf,
    wv_buf,
    gain_ref,
    query_ref,
    gate_ref,
    norm_buf,
    staging,
    gates_in,
    own_parts,
    plane_parts,
    merged_parts,
    line_parts,
    finals,
    tok_sem,
    ramp_sem,
    w_sem,
    send_sem,
    recv_sem,
    gate_send_sem,
    gate_recv_sem,
    stage_send_sem,
    stage_recv_sem,
    own_sem,
):
    sp_count, tp_count, seqs, heads, positions, width = sizes
    devices = sp_count * tp_count
    classes, halves = sp_count // seqs, tp_count // heads
    piece = positions // (classes * halves)
    sp, tp = lax.axis_index("sp"), lax.axis_index("tp")
    me = sp * tp_count + tp
    seq_me, head_me = sp // classes, tp // halves
    tile = min(TILE, positions)
    tiles = positions // tile
    ramp = tile // 2
    window = max(piece, 128)
    edge = is_edge(seq_me, seqs)
    early = min(tiles + max(tiles // 2, 1), (seqs - 1) * tiles)
    last = (seqs - 1) * tiles

    def place(other):
        return {"sp": other // tp_count, "tp": other % tp_count}

    def for_others(body):
        def visit(other, carry):
            @pl.when(other != me)
            def _():
                body(other)

            return carry

        lax.fori_loop(0, devices, visit, 0)

    def for_line(body):
        def visit(other, carry):
            @pl.when(other != sp)
            def _():
                body(other)

            return carry

        lax.fori_loop(0, sp_count, visit, 0)

    def for_plane(body):
        def visit(other, carry):
            @pl.when(other != tp)
            def _():
                body(other)

            return carry

        lax.fori_loop(0, tp_count, visit, 0)

    def rows_copy(step, row0, rows, sem):
        seq = sequence_at(step, seq_me, seqs)
        part = pl.ds(row0, rows)
        return pltpu.make_async_copy(tokens_hbm.at[seq, part, :], tok_buf.at[step, part, :], sem)

    def ramp_copy(part):
        return rows_copy(0, part * ramp, ramp, ramp_sem.at[part])

    def token_copy(index):
        step, part = index // tiles, index % tiles
        row0 = pl.multiple_of(part * tile, tile)
        return rows_copy(step, row0, tile, tok_sem.at[step, part])

    k_copy = pltpu.make_async_copy(wk_hbm, wk_buf, w_sem.at[0])
    v_copy = pltpu.make_async_copy(wv_hbm, wv_buf, w_sem.at[1])
    gain_copy = pltpu.make_async_copy(gain_hbm, gain_ref, w_sem.at[2])
    query_copy = pltpu.make_async_copy(query_hbm, query_ref, w_sem.at[3])
    gate_copy = pltpu.make_async_copy(gate_hbm, gate_ref, w_sem.at[4])
    ramp_copy(0).start()
    gain_copy.start()
    k_copy.start()
    v_copy.start()
    ramp_copy(1).start()

    barrier = pltpu.get_barrier_semaphore()

    def greet(other):
        pl.semaphore_signal(barrier, inc=1, device_id=place(other), device_id_type=MESH)

    for_others(greet)
    gate_copy.start()
    query_copy.start()

    def normalize(step, row0, rows):
        gain = gain_ref[...]
        for piece_row in range(0, rows, NORM_ROWS):
            block = tok_buf[step, pl.ds(row0 + piece_row, NORM_ROWS), :].astype(jnp.float32)
            mean = jnp.mean(block * block, axis=-1, keepdims=True)
            normed = block * lax.rsqrt(mean + NORM_FLOOR) * gain
            norm_buf[pl.ds(piece_row, NORM_ROWS), :] = normed.astype(jnp.bfloat16)

    def multiply(step, row0, rows):
        seq = sequence_at(step, seq_me, seqs)
        normed_tile = norm_buf[:rows, :]
        keys = jnp.dot(normed_tile, wk_buf[...], preferred_element_type=jnp.float32)
        values = jnp.dot(normed_tile, wv_buf[...], preferred_element_type=jnp.float32)
        keys = keys.astype(jnp.bfloat16)
        values = values.astype(jnp.bfloat16)
        for head in range(heads):
            cols = slice(head * HD, (head + 1) * HD)
            both = jnp.concatenate([keys[:, cols], values[:, cols]], axis=1)
            staging[seq * heads + head, pl.ds(row0, rows), :] = both

    def gate_window(other):
        start = pl.multiple_of(other * piece // window * window, window)
        return gate_ref.at[:, pl.ds(start, window)]

    def send_gate(other):
        pltpu.make_async_remote_copy(
            src_ref=gate_window(other),
            dst_ref=gates_in.at[me],
            send_sem=gate_send_sem,
            recv_sem=gate_recv_sem,
            device_id=place(other),
            device_id_type=MESH,
        ).start()

    def send_rows(step, row0, rows):
        seq = sequence_at(step, seq_me, seqs)
        sub = min(piece, rows)
        for head in range(heads):
            for piece_row in range(0, rows, sub):
                row = pl.multiple_of(row0 + piece_row, sub)
                slot = row // piece
                to_sp = seq * classes + slot // halves
                to_tp = head * halves + slot % halves
                dest = to_sp * tp_count + to_tp
                landing = pl.multiple_of(me * piece + row % piece, sub)
                source = staging.at[seq * heads + head, pl.ds(row, sub), :]
                target = cache_ref.at[pl.ds(landing, sub), :]

                @pl.when(dest != me)
                def _():
                    pltpu.make_async_remote_copy(
                        src_ref=source,
                        dst_ref=target,
                        send_sem=send_sem,
                        recv_sem=recv_sem,
                        device_id={"sp": to_sp, "tp": to_tp},
                        device_id_type=MESH,
                    ).start()

                @pl.when(dest == me)
                def _():
                    pltpu.make_async_copy(source, target, own_sem).start()

    def send_tiles(first, last):
        def visit(index, carry):
            send_rows(index // tiles, index % tiles * tile, tile)
            return carry

        lax.fori_loop(first, last, visit, 0)

    def wait_bytes(ref, sem):
        pltpu.make_async_copy(ref, ref, sem).wait()

    gain_copy.wait()
    ramp_copy(0).wait()
    normalize(0, 0, ramp)
    k_copy.wait()
    v_copy.wait()
    for index in range(1, seqs * tiles):
        token_copy(index).start()
    multiply(0, 0, ramp)
    gate_copy.wait()
    pl.semaphore_wait(barrier, devices - 1)
    for_others(send_gate)
    send_rows(0, 0, ramp)
    ramp_copy(1).wait()
    normalize(0, ramp, ramp)
    multiply(0, ramp, ramp)
    send_rows(0, ramp, ramp)

    def project(index, carry):
        step, part = index // tiles, index % tiles
        row0 = pl.multiple_of(part * tile, tile)
        token_copy(index).wait()
        normalize(step, row0, tile)
        multiply(step, row0, tile)

        @pl.when((index < tiles) | (edge & (index < early)))
        def _():
            send_rows(step, row0, tile)

        return carry

    lax.fori_loop(1, seqs * tiles, project, 0)

    query_copy.wait()
    group = query_ref.shape[2]
    gates_in[me] = gate_ref[:, pl.ds(pl.multiple_of(me * piece // window * window, window), window)]
    other_gates = gates_in.at[pl.ds(0, devices - 1)]
    wait_bytes(other_gates, gate_recv_sem)
    lane = lax.broadcasted_iota(jnp.int32, (group, 2 * HD), 1)
    line = lax.broadcasted_iota(jnp.int32, (group, 2 * HD), 0)
    half = group // 2

    def pack(ref, top, total, out):
        folded = jnp.concatenate([out[:half], out[half:]], axis=1)
        stats = jnp.where(lane == line, top, 0.0) + jnp.where(lane == line + group, total, 0.0)
        for k in range(half):
            ref[:, k * 2 * HD : (k + 1) * 2 * HD] = folded[k : k + 1]
        ref[:, half * 2 * HD :] = jnp.sum(stats, axis=0, keepdims=True)

    def unpack(ref):
        rows = [ref[:, k * 2 * HD : (k + 1) * 2 * HD] for k in range(half + 1)]
        out = jnp.concatenate([r[:, :HD] for r in rows[:half]] + [r[:, HD:] for r in rows[:half]])
        top = jnp.sum(jnp.where(lane == line, rows[half], 0.0), axis=1, keepdims=True)
        total = jnp.sum(jnp.where(lane == line + group, rows[half], 0.0), axis=1, keepdims=True)
        return top, total, out

    def merge(left, right):
        best = jnp.maximum(left[0], right[0])
        scale_left, scale_right = jnp.exp(left[0] - best), jnp.exp(right[0] - best)
        total = left[1] * scale_left + right[1] * scale_right
        return best, total, left[2] * scale_left + right[2] * scale_right

    def attend(seq, carry):
        for head in range(heads):
            query = query_ref[seq, head]
            query = jnp.concatenate([query, jnp.zeros_like(query)], axis=1)
            for slot in range(classes * halves):
                to_sp = seq * classes + slot // halves
                to_tp = head * halves + slot % halves
                block = staging[seq * heads + head, slot * piece : (slot + 1) * piece, :]
                gates = gates_in[to_sp * tp_count + to_tp]
                choices = [gates[:, k * piece : (k + 1) * piece] for k in range(window // piece)]
                gate = choices[0]
                for k in range(1, len(choices)):
                    gate = jnp.where(me % (window // piece) == k, choices[k], gate)
                scores = lax.dot_general(
                    query, block, (((1,), (1,)), ((), ())), preferred_element_type=jnp.float32
                )
                scores = scores * HD ** (-0.5) - gate
                top = jnp.max(scores, axis=1, keepdims=True)
                weights = jnp.exp(scores - top)
                total = jnp.sum(weights, axis=1, keepdims=True)
                first = weights.astype(jnp.bfloat16).astype(jnp.float32)
                rest = weights - first
                second = rest.astype(jnp.bfloat16).astype(jnp.float32)
                stacked = jnp.concatenate([first, second, rest - second], axis=0)
                summed = jnp.dot(
                    stacked.astype(jnp.bfloat16), block, preferred_element_type=jnp.float32
                )
                summed = summed[:group] + summed[group : 2 * group] + summed[2 * group :]
                pack(own_parts.at[to_tp, to_sp], top, total, summed[:, HD:])
        return carry

    lax.fori_loop(0, seqs, attend, 0)

    def exchange(stage, source, target, device):
        pltpu.make_async_remote_copy(
            src_ref=source,
            dst_ref=target,
            send_sem=stage_send_sem.at[stage],
            recv_sem=stage_recv_sem.at[stage],
            device_id=device,
            device_id_type=MESH,
        ).start()

    plane = plane_parts.at[pl.ds(0, tp_count - 1)]
    along = line_parts.at[pl.ds(0, sp_count - 1)]

    for_plane(lambda t: exchange(0, own_parts.at[t], plane_parts.at[tp], {"tp": t}))
    plane_parts[tp] = own_parts[tp]
    wait_bytes(plane, stage_recv_sem.at[0])

    def merge_plane(s, carry):
        merged = functools.reduce(merge, [unpack(plane_parts.at[t, s]) for t in range(tp_count)])
        pack(merged_parts.at[s], *merged)
        return carry

    lax.fori_loop(0, sp_count, merge_plane, 0)
    for_line(lambda s: exchange(1, merged_parts.at[s], line_parts.at[sp], {"sp": s}))
    line_parts[sp] = merged_parts[sp]

    @pl.when(~edge)
    def _():
        send_tiles(tiles, early)

    wait_bytes(along, stage_recv_sem.at[1])
    merged = lax.fori_loop(
        1, sp_count, lambda s, kept: merge(kept, unpack(line_parts.at[s])), unpack(line_parts.at[0])
    )
    pack(finals.at[tp, sp], *merged)
    mine = finals.at[tp, sp]
    for_line(lambda s: exchange(2, mine, mine, {"sp": s}))

    @pl.when(~edge)
    def _():
        send_tiles(early, last)

    wait_bytes(along, stage_recv_sem.at[2])
    for_plane(lambda t: exchange(3, finals.at[tp], finals.at[tp], {"tp": t}))

    @pl.when(edge)
    def _():
        send_tiles(early, last)

    send_tiles(last, seqs * tiles)
    wait_bytes(plane, stage_recv_sem.at[3])
    for seq in range(seqs):
        for head in range(heads):
            slots = [
                unpack(finals.at[head * halves + b, seq * classes + c])
                for c in range(classes)
                for b in range(halves)
            ]
            _, total, out = functools.reduce(merge, slots)
            read_ref[seq, pl.ds(head * group, group), :] = out / total
    wait_bytes(other_gates, gate_send_sem)
    wait_bytes(plane, stage_send_sem.at[0])
    wait_bytes(along, stage_send_sem.at[1])
    wait_bytes(along, stage_send_sem.at[2])
    wait_bytes(plane, stage_send_sem.at[3])
    wait_bytes(cache_ref.at[pl.ds(0, piece), :], own_sem)
    sent = cache_ref.at[pl.ds(0, (devices - 1) * piece), :]
    wait_bytes(sent, send_sem)
    wait_bytes(sent, recv_sem)


def settle(cache_in, read_in, cache_out, read_out, sems):
    copies = [
        pltpu.make_async_copy(cache_in, cache_out, sems.at[0]),
        pltpu.make_async_copy(read_in, read_out, sems.at[1]),
    ]
    for copy in copies:
        copy.start()
    for copy in copies:
        copy.wait()


def solution(mesh):
    sp_count, tp_count = mesh.shape["sp"], mesh.shape["tp"]
    devices = sp_count * tp_count

    def shards(tokens, norm_gain, w_key, w_value, new_query, cum_gate):
        seqs, positions, width = tokens.shape
        heads = w_key.shape[1] // HD
        columns = w_key.shape[1]
        query_heads = new_query.shape[1]
        group = query_heads // heads
        length = cum_gate.shape[-1]
        tile = min(TILE, positions)
        part = (group // 2 + 1) * 2 * HD
        sizes = (sp_count, tp_count, seqs, heads, positions, width)
        vmem = pl.BlockSpec(memory_space=pltpu.VMEM)
        anywhere = pl.BlockSpec(memory_space=pltpu.HBM)
        cache, first_read = pl.pallas_call(
            functools.partial(kernel, sizes),
            out_shape=(
                pltpu.VMEM((length, 2 * HD), jnp.bfloat16),
                pltpu.VMEM((seqs, query_heads, HD), jnp.float32),
            ),
            in_specs=[anywhere] * 6,
            out_specs=(vmem, vmem),
            scratch_shapes=[
                pltpu.VMEM((seqs, positions, width), jnp.bfloat16),
                pltpu.VMEM((width, columns), jnp.bfloat16),
                pltpu.VMEM((width, columns), jnp.bfloat16),
                pltpu.VMEM((1, width), jnp.float32),
                pltpu.VMEM((seqs, heads, group, HD), jnp.bfloat16),
                pltpu.VMEM((1, length), jnp.float32),
                pltpu.VMEM((tile, width), jnp.bfloat16),
                pltpu.VMEM((seqs * heads, positions, 2 * HD), jnp.bfloat16),
                pltpu.VMEM((devices, 1, max(length // devices, 128)), jnp.float32),
                pltpu.VMEM((tp_count, sp_count, 1, part), jnp.float32),
                pltpu.VMEM((tp_count, sp_count, 1, part), jnp.float32),
                pltpu.VMEM((sp_count, 1, part), jnp.float32),
                pltpu.VMEM((sp_count, 1, part), jnp.float32),
                pltpu.VMEM((tp_count, sp_count, 1, part), jnp.float32),
                pltpu.SemaphoreType.DMA((seqs, positions // tile)),
                pltpu.SemaphoreType.DMA((2,)),
                pltpu.SemaphoreType.DMA((5,)),
                *[pltpu.SemaphoreType.DMA] * 4,
                pltpu.SemaphoreType.DMA((4,)),
                pltpu.SemaphoreType.DMA((4,)),
                pltpu.SemaphoreType.DMA,
            ],
            compiler_params=pltpu.CompilerParams(
                collective_id=0, has_side_effects=True, vmem_limit_bytes=VMEM_BYTES
            ),
        )(
            tokens,
            norm_gain.reshape(1, width),
            w_key,
            w_value,
            new_query.reshape(seqs, heads, group, HD),
            cum_gate.reshape(1, length),
        )
        cache, first_read = pl.pallas_call(
            settle,
            out_shape=(
                jax.ShapeDtypeStruct(cache.shape, cache.dtype),
                jax.ShapeDtypeStruct(first_read.shape, first_read.dtype),
            ),
            in_specs=[vmem] * 2,
            out_specs=(anywhere, anywhere),
            scratch_shapes=[pltpu.SemaphoreType.DMA((2,))],
            compiler_params=pltpu.CompilerParams(vmem_limit_bytes=VMEM_BYTES),
        )(
            pltpu.with_memory_space_constraint(cache, pltpu.VMEM),
            pltpu.with_memory_space_constraint(first_read, pltpu.VMEM),
        )
        return cache.reshape(1, 1, length, 2 * HD), first_read

    in_specs = (
        P("gr", ("sp", "tp"), None),
        P(),
        P(),
        P(),
        P("gr", None, None),
        P(("gr", "sp"), "tp", None),
    )
    out_specs = (P(("gr", "sp"), "tp", None, None), P("gr", None, None))
    return jax.shard_map(shards, mesh=mesh, in_specs=in_specs, out_specs=out_specs, check_vma=False)
```

time: 57.2 us -> 54.2 us (0.948)
  Pallas kernels: 56 us -> 53.4 us
    pallas_call x1, Pallas kernels: 54.7 us -> 52 us  [shards(): pl.pallas_call(functools.partial(kernel, sizes), out_shape=(pltpu.VMEM((l...]
where the time goes in v2:
time: 54.2 us; the launch traced here: 54 us
  Pallas kernels  53.4 us (99%)
  between operations  0.64 us (1%)
    pallas_call x1, Pallas kernels, shards(): pl.pallas_call(functools.partial(kernel, sizes), out_shape=(pltpu.VMEM((l...  52 us
    pallas_call x1, Pallas kernels, shards(): pl.pallas_call(settle, out_shape=(jax.ShapeDtypeStruct(cache.shape, cache...  1.34 us

profile of v2, /device:TPU:13, one launch (start us, length us, event | category | flops | bytes accessed | tf_op | source)
XLA Modules:
  0.0 54.0 jit_solution(4590566768815616497)
XLA Ops:
  0.6 52.0 %shard_map.77 = (bf16[8192,128]{1,0:T(8,128)(2,1)S(1)}, f32[4,32,64]{2,1,0:T(8,128)S(1)}) custom-call(bf16[4,512,2048]{2,1,0:T(8,128)(2,1)} %tokens_hbm.1, f32[1,2048]{1,0:T(1,128)} %bitcast.6, bf16[2048,256]{1,0:T(8,128)(2,1)} %wk_hbm.1, bf16[2048,256]{1,0:T(8,128)(2,1)} %wv_hbm.1, bf16[4,4,8,64]{3,2,1,0:T(8,128)(2,1)} %bitcast.4, f32[1,8192]{1,0:T(1,128)} %bitcast.5), custom_call_target="tpu_custom_call" | custom-call | tf_op jit(solution)/shard_map/pallas_call | solution.py:415
  52.7 1.3 %shard_map.78 = (bf16[8192,128]{1,0:T(8,128)(2,1)}, f32[4,32,64]{2,1,0:T(8,128)}) custom-call(bf16[8192,128]{1,0:T(8,128)(2,1)S(1)} %get-tuple-element.6.cache_in, f32[4,32,64]{2,1,0:T(8,128)S(1)} %get-tuple-element.7.read_in), custom_call_target="tpu_custom_call" | custom-call | tf_op jit(solution)/shard_map/pallas_call | solution.py:457

commit v3 on v2

--- a/solution.py
+++ b/solution.py
@@ -17,7 +17,7 @@
 
 
 def is_edge(own, count):
-    return (own == 0) | (own == count - 1)
+    return (own == 0) | (own == count - 1) | (count < 4)
 
 
 def sequence_at(step, own, count):
@@ -65,6 +65,7 @@
     stage_send_sem,
     stage_recv_sem,
     own_sem,
+    ready,
 ):
     sp_count, tp_count, seqs, heads, positions, width = sizes
     devices = sp_count * tp_count
@@ -75,11 +76,14 @@
     seq_me, head_me = sp // classes, tp // halves
     tile = min(TILE, positions)
     tiles = positions // tile
-    ramp = tile // 2
+    half_tile = tile // 2
+    ramp = tile // 4
     window = max(piece, 128)
     edge = is_edge(seq_me, seqs)
-    early = min(tiles + max(tiles // 2, 1), (seqs - 1) * tiles)
+    edge_devices = devices if seqs < 4 else 2 * classes * tp_count
+    lead = max(tiles // 2, 1)
     last = (seqs - 1) * tiles
+    units = seqs * tiles
 
     def place(other):
         return {"sp": other // tp_count, "tp": other % tp_count}
@@ -114,18 +118,26 @@
 
         lax.fori_loop(0, tp_count, visit, 0)
 
-    def rows_copy(step, row0, rows, sem):
-        seq = sequence_at(step, seq_me, seqs)
-        part = pl.ds(row0, rows)
-        return pltpu.make_async_copy(tokens_hbm.at[seq, part, :], tok_buf.at[step, part, :], sem)
+    def unit_at(unit):
+        ahead = unit == 0
+        step = jnp.where(ahead, 1, jnp.where(unit <= tiles, 0, unit // tiles))
+        part = jnp.where(ahead, 0, jnp.where(unit <= tiles, unit - 1, unit % tiles))
+        step = jnp.where(edge, unit // tiles, step)
+        part = jnp.where(edge, unit % tiles, part)
+        return sequence_at(step, seq_me, seqs), pl.multiple_of(part * tile, tile)
+
+    def rows_copy(unit, row, rows, sem):
+        seq, row0 = unit_at(unit)
+        source = tokens_hbm.at[seq, pl.ds(row0 + row, rows), :]
+        return pltpu.make_async_copy(source, tok_buf.at[unit, pl.ds(row, rows), :], sem)
 
     def ramp_copy(part):
-        return rows_copy(0, part * ramp, ramp, ramp_sem.at[part])
-
-    def token_copy(index):
-        step, part = index // tiles, index % tiles
-        row0 = pl.multiple_of(part * tile, tile)
-        return rows_copy(step, row0, tile, tok_sem.at[step, part])
+        if part:
+            return rows_copy(0, ramp, tile - ramp, ramp_sem.at[1])
+        return rows_copy(0, 0, ramp, ramp_sem.at[0])
+
+    def token_copy(unit):
+        return rows_copy(unit, 0, tile, tok_sem.at[unit])
 
     k_copy = pltpu.make_async_copy(wk_hbm, wk_buf, w_sem.at[0])
     v_copy = pltpu.make_async_copy(wv_hbm, wv_buf, w_sem.at[1])
@@ -134,29 +146,50 @@
     gate_copy = pltpu.make_async_copy(gate_hbm, gate_ref, w_sem.at[4])
     ramp_copy(0).start()
     gain_copy.start()
+    gate_copy.start()
     k_copy.start()
     v_copy.start()
     ramp_copy(1).start()
 
     barrier = pltpu.get_barrier_semaphore()
 
+    def on_edge(other):
+        return is_edge(other // tp_count // classes, seqs)
+
     def greet(other):
         pl.semaphore_signal(barrier, inc=1, device_id=place(other), device_id_type=MESH)
 
-    for_others(greet)
-    gate_copy.start()
+    def greet_edge(other):
+        @pl.when(on_edge(other))
+        def _():
+            greet(other)
+
+    def answer(other):
+        @pl.when(~on_edge(other))
+        def _():
+            pl.semaphore_signal(ready, inc=1, device_id=place(other), device_id_type=MESH)
+
+    @pl.when(edge)
+    def _():
+        for_others(greet_edge)
+
+    @pl.when(~edge)
+    def _():
+        for_others(greet)
+
     query_copy.start()
 
-    def normalize(step, row0, rows):
+    def normalize(unit, row, rows):
         gain = gain_ref[...]
         for piece_row in range(0, rows, NORM_ROWS):
-            block = tok_buf[step, pl.ds(row0 + piece_row, NORM_ROWS), :].astype(jnp.float32)
+            block = tok_buf[unit, row + piece_row : row + piece_row + NORM_ROWS, :]
+            block = block.astype(jnp.float32)
             mean = jnp.mean(block * block, axis=-1, keepdims=True)
             normed = block * lax.rsqrt(mean + NORM_FLOOR) * gain
             norm_buf[pl.ds(piece_row, NORM_ROWS), :] = normed.astype(jnp.bfloat16)
 
-    def multiply(step, row0, rows):
-        seq = sequence_at(step, seq_me, seqs)
+    def multiply(unit, row, rows):
+        seq, row0 = unit_at(unit)
         normed_tile = norm_buf[:rows, :]
         keys = jnp.dot(normed_tile, wk_buf[...], preferred_element_type=jnp.float32)
         values = jnp.dot(normed_tile, wv_buf[...], preferred_element_type=jnp.float32)
@@ -165,7 +198,7 @@
         for head in range(heads):
             cols = slice(head * HD, (head + 1) * HD)
             both = jnp.concatenate([keys[:, cols], values[:, cols]], axis=1)
-            staging[seq * heads + head, pl.ds(row0, rows), :] = both
+            staging[seq * heads + head, pl.ds(pl.multiple_of(row0 + row, ramp), rows), :] = both
 
     def gate_window(other):
         start = pl.multiple_of(other * piece // window * window, window)
@@ -181,8 +214,17 @@
             device_id_type=MESH,
         ).start()
 
-    def send_rows(step, row0, rows):
-        seq = sequence_at(step, seq_me, seqs)
+    def send_gate_if(chosen):
+        def visit(other):
+            @pl.when(chosen(other))
+            def _():
+                send_gate(other)
+
+        for_others(visit)
+
+    def send_rows(unit, start, rows):
+        seq, row0 = unit_at(unit)
+        row0 = row0 + start
         sub = min(piece, rows)
         for head in range(heads):
             for piece_row in range(0, rows, sub):
@@ -210,9 +252,9 @@
                 def _():
                     pltpu.make_async_copy(source, target, own_sem).start()
 
-    def send_tiles(first, last):
-        def visit(index, carry):
-            send_rows(index // tiles, index % tiles * tile, tile)
+    def send_units(first, last, start=0, rows=tile):
+        def visit(unit, carry):
+            send_rows(unit, start, rows)
             return carry
 
         lax.fori_loop(first, last, visit, 0)
@@ -223,34 +265,56 @@
     gain_copy.wait()
     ramp_copy(0).wait()
     normalize(0, 0, ramp)
+    gate_copy.wait()
+
+    @pl.when(edge)
+    def _():
+        pl.semaphore_wait(barrier, devices - 1)
+        for_others(answer)
+        for_others(send_gate)
+
+    @pl.when(~edge)
+    def _():
+        pl.semaphore_wait(barrier, devices - edge_devices - 1)
+        send_gate_if(lambda other: ~on_edge(other))
+
     k_copy.wait()
     v_copy.wait()
-    for index in range(1, seqs * tiles):
-        token_copy(index).start()
+    for unit in range(1, units):
+        token_copy(unit).start()
     multiply(0, 0, ramp)
-    gate_copy.wait()
-    pl.semaphore_wait(barrier, devices - 1)
-    for_others(send_gate)
     send_rows(0, 0, ramp)
     ramp_copy(1).wait()
-    normalize(0, ramp, ramp)
-    multiply(0, ramp, ramp)
+    normalize(0, ramp, tile - ramp)
+    multiply(0, ramp, tile - ramp)
     send_rows(0, ramp, ramp)
-
-    def project(index, carry):
-        step, part = index // tiles, index % tiles
-        row0 = pl.multiple_of(part * tile, tile)
-        token_copy(index).wait()
-        normalize(step, row0, tile)
-        multiply(step, row0, tile)
-
-        @pl.when((index < tiles) | (edge & (index < early)))
+    send_rows(0, half_tile, half_tile)
+
+    def project(unit, carry):
+        token_copy(unit).wait()
+        normalize(unit, 0, tile)
+        multiply(unit, 0, tile)
+
+        @pl.when((unit == 1) & ~edge)
         def _():
-            send_rows(step, row0, tile)
+            pl.semaphore_wait(ready, edge_devices)
+            send_gate_if(on_edge)
+
+        @pl.when((unit < jnp.where(edge, lead, tiles)) | (edge & (unit // lead * lead == tiles)))
+        def _():
+            send_rows(unit, 0, tile)
+
+        @pl.when(edge & (unit == tiles + lead))
+        def _():
+            send_units(lead, tiles)
+
+        @pl.when(~edge & (unit == tiles + 1))
+        def _():
+            send_units(tiles, 2 * tiles - 1, 0, half_tile)
 
         return carry
 
-    lax.fori_loop(1, seqs * tiles, project, 0)
+    lax.fori_loop(1, units, project, 0)
 
     query_copy.wait()
     group = query_ref.shape[2]
@@ -342,8 +406,9 @@
 
     @pl.when(~edge)
     def _():
-        send_tiles(tiles, early)
-
+        send_units(tiles, 2 * tiles - 1, half_tile, half_tile)
+
+    send_units(last, units)
     wait_bytes(along, stage_recv_sem.at[1])
     merged = lax.fori_loop(
         1, sp_count, lambda s, kept: merge(kept, unpack(line_parts.at[s])), unpack(line_parts.at[0])
@@ -354,16 +419,15 @@
 
     @pl.when(~edge)
     def _():
-        send_tiles(early, last)
+        send_units(2 * tiles - 1, last)
 
     wait_bytes(along, stage_recv_sem.at[2])
     for_plane(lambda t: exchange(3, finals.at[tp], finals.at[tp], {"tp": t}))
 
     @pl.when(edge)
     def _():
-        send_tiles(early, last)
-
-    send_tiles(last, seqs * tiles)
+        send_units(tiles + lead, last)
+
     wait_bytes(plane, stage_recv_sem.at[3])
     for seq in range(seqs):
         for head in range(heads):
@@ -421,7 +485,7 @@
             in_specs=[anywhere] * 6,
             out_specs=(vmem, vmem),
             scratch_shapes=[
-                pltpu.VMEM((seqs, positions, width), jnp.bfloat16),
+                pltpu.VMEM((seqs * positions // tile, tile, width), jnp.bfloat16),
                 pltpu.VMEM((width, columns), jnp.bfloat16),
                 pltpu.VMEM((width, columns), jnp.bfloat16),
                 pltpu.VMEM((1, width), jnp.float32),
@@ -435,13 +499,14 @@
                 pltpu.VMEM((sp_count, 1, part), jnp.float32),
                 pltpu.VMEM((sp_count, 1, part), jnp.float32),
                 pltpu.VMEM((tp_count, sp_count, 1, part), jnp.float32),
-                pltpu.SemaphoreType.DMA((seqs, positions // tile)),
+                pltpu.SemaphoreType.DMA((seqs * positions // tile,)),
                 pltpu.SemaphoreType.DMA((2,)),
                 pltpu.SemaphoreType.DMA((5,)),
                 *[pltpu.SemaphoreType.DMA] * 4,
                 pltpu.SemaphoreType.DMA((4,)),
                 pltpu.SemaphoreType.DMA((4,)),
                 pltpu.SemaphoreType.DMA,
+                pltpu.SemaphoreType.REGULAR,
             ],
             compiler_params=pltpu.CompilerParams(
                 collective_id=0, has_side_effects=True, vmem_limit_bytes=VMEM_BYTES

time: 54.2 us -> 53.4 us (0.985)
  Pallas kernels: 53.4 us -> 52.6 us
    pallas_call x1, Pallas kernels: 52 us -> 51.3 us  [shards(): pl.pallas_call(functools.partial(kernel, sizes), out_shape=(pltpu.VMEM((l...]
where the time goes in v3:
time: 53.4 us; the launch traced here: 53.2 us
  Pallas kernels  52.6 us (99%)
  between operations  0.64 us (1%)
    pallas_call x1, Pallas kernels, shards(): pl.pallas_call(functools.partial(kernel, sizes), out_shape=(pltpu.VMEM((l...  51.3 us
    pallas_call x1, Pallas kernels, shards(): pl.pallas_call(settle, out_shape=(jax.ShapeDtypeStruct(cache.shape, cache...  1.34 us

profile of v3, /device:TPU:13, one launch (start us, length us, event | category | flops | bytes accessed | tf_op | source)
XLA Modules:
  0.0 53.2 jit_solution(11943395440105802946)
XLA Ops:
  0.6 51.3 %shard_map.77 = (bf16[8192,128]{1,0:T(8,128)(2,1)S(1)}, f32[4,32,64]{2,1,0:T(8,128)S(1)}) custom-call(bf16[4,512,2048]{2,1,0:T(8,128)(2,1)} %tokens_hbm.1, f32[1,2048]{1,0:T(1,128)} %bitcast.6, bf16[2048,256]{1,0:T(8,128)(2,1)} %wk_hbm.1, bf16[2048,256]{1,0:T(8,128)(2,1)} %wv_hbm.1, bf16[4,4,8,64]{3,2,1,0:T(8,128)(2,1)} %bitcast.4, f32[1,8192]{1,0:T(1,128)} %bitcast.5), custom_call_target="tpu_custom_call" | custom-call | tf_op jit(solution)/shard_map/pallas_call | solution.py:479
  51.9 1.3 %shard_map.78 = (bf16[8192,128]{1,0:T(8,128)(2,1)}, f32[4,32,64]{2,1,0:T(8,128)}) custom-call(bf16[8192,128]{1,0:T(8,128)(2,1)S(1)} %get-tuple-element.6.cache_in, f32[4,32,64]{2,1,0:T(8,128)S(1)} %get-tuple-element.7.read_in), custom_call_target="tpu_custom_call" | custom-call | tf_op jit(solution)/shard_map/pallas_call | solution.py:522

commit v4 on v3

--- a/solution.py
+++ b/solution.py
@@ -16,8 +16,12 @@
 VMEM_BYTES = 60_000_000
 
 
+def has_middle(count):
+    return count >= 4 and count % 2 == 0
+
+
 def is_edge(own, count):
-    return (own == 0) | (own == count - 1) | (count < 4)
+    return (own == 0) | (own == count - 1) | (not has_middle(count))
 
 
 def sequence_at(step, own, count):
@@ -80,7 +84,7 @@
     ramp = tile // 4
     window = max(piece, 128)
     edge = is_edge(seq_me, seqs)
-    edge_devices = devices if seqs < 4 else 2 * classes * tp_count
+    edge_devices = 2 * classes * tp_count if has_middle(seqs) else devices
     lead = max(tiles // 2, 1)
     last = (seqs - 1) * tiles
     units = seqs * tiles
@@ -144,39 +148,41 @@
     gain_copy = pltpu.make_async_copy(gain_hbm, gain_ref, w_sem.at[2])
     query_copy = pltpu.make_async_copy(query_hbm, query_ref, w_sem.at[3])
     gate_copy = pltpu.make_async_copy(gate_hbm, gate_ref, w_sem.at[4])
+    def on_edge(other):
+        return is_edge(other // tp_count // classes, seqs)
+
+    def greet(other):
+        pl.semaphore_signal(barrier, inc=1, device_id=place(other), device_id_type=MESH)
+
+    def answer(other):
+        @pl.when(~on_edge(other))
+        def _():
+            pl.semaphore_signal(ready, inc=1, device_id=place(other), device_id_type=MESH)
+
+    upper = seq_me >= seqs // 2
+    plane_size = classes * tp_count
+    across_first = jnp.where(upper, 1, seqs // 2) * plane_size
+    across_count = (seqs // 2 - 1) * plane_size
+    barrier = pltpu.get_barrier_semaphore()
+
+    def is_across(other):
+        return (other >= across_first) & (other < across_first + across_count)
+
+    def greet_across(index, carry):
+        greet(across_first + index)
+        return carry
+
+    @pl.when(~edge)
+    def _():
+        lax.fori_loop(0, across_count, greet_across, 0)
+
     ramp_copy(0).start()
     gain_copy.start()
     gate_copy.start()
     k_copy.start()
     v_copy.start()
-    ramp_copy(1).start()
-
-    barrier = pltpu.get_barrier_semaphore()
-
-    def on_edge(other):
-        return is_edge(other // tp_count // classes, seqs)
-
-    def greet(other):
-        pl.semaphore_signal(barrier, inc=1, device_id=place(other), device_id_type=MESH)
-
-    def greet_edge(other):
-        @pl.when(on_edge(other))
-        def _():
-            greet(other)
-
-    def answer(other):
-        @pl.when(~on_edge(other))
-        def _():
-            pl.semaphore_signal(ready, inc=1, device_id=place(other), device_id_type=MESH)
-
-    @pl.when(edge)
-    def _():
-        for_others(greet_edge)
-
-    @pl.when(~edge)
-    def _():
-        for_others(greet)
-
+
+    for_others(lambda other: pl.when(on_edge(other))(lambda: greet(other)))
     query_copy.start()
 
     def normalize(unit, row, rows):
@@ -262,27 +268,30 @@
     def wait_bytes(ref, sem):
         pltpu.make_async_copy(ref, ref, sem).wait()
 
+    def open_links(chosen):
+        @pl.when(chosen & edge)
+        def _():
+            pl.semaphore_wait(barrier, devices - 1)
+            for_others(answer)
+            for_others(send_gate)
+
+        @pl.when(chosen & ~edge)
+        def _():
+            pl.semaphore_wait(barrier, across_count)
+            send_gate_if(is_across)
+
+    gate_copy.wait()
+    open_links(upper)
     gain_copy.wait()
     ramp_copy(0).wait()
     normalize(0, 0, ramp)
-    gate_copy.wait()
-
-    @pl.when(edge)
-    def _():
-        pl.semaphore_wait(barrier, devices - 1)
-        for_others(answer)
-        for_others(send_gate)
-
-    @pl.when(~edge)
-    def _():
-        pl.semaphore_wait(barrier, devices - edge_devices - 1)
-        send_gate_if(lambda other: ~on_edge(other))
-
+    ramp_copy(1).start()
     k_copy.wait()
     v_copy.wait()
     for unit in range(1, units):
         token_copy(unit).start()
     multiply(0, 0, ramp)
+    open_links(~upper)
     send_rows(0, 0, ramp)
     ramp_copy(1).wait()
     normalize(0, ramp, tile - ramp)
@@ -298,7 +307,7 @@
         @pl.when((unit == 1) & ~edge)
         def _():
             pl.semaphore_wait(ready, edge_devices)
-            send_gate_if(on_edge)
+            send_gate_if(lambda other: ~is_across(other))
 
         @pl.when((unit < jnp.where(edge, lead, tiles)) | (edge & (unit // lead * lead == tiles)))
         def _():

time: 53.4 us -> 53 us (level)
  no operation moved by 1% of the time
where the time goes in v4:
time: 53 us; the launch traced here: 52.8 us
  Pallas kernels  52.2 us (98%)
  between operations  0.64 us (1%)
    pallas_call x1, Pallas kernels, shards(): pl.pallas_call(functools.partial(kernel, sizes), out_shape=(pltpu.VMEM((l...  50.8 us
    pallas_call x1, Pallas kernels, shards(): pl.pallas_call(settle, out_shape=(jax.ShapeDtypeStruct(cache.shape, cache...  1.34 us

profile of v4, /device:TPU:13, one launch (start us, length us, event | category | flops | bytes accessed | tf_op | source)
XLA Modules:
  0.0 52.8 jit_solution(5156411222109115944)
XLA Ops:
  0.6 50.8 %shard_map.77 = (bf16[8192,128]{1,0:T(8,128)(2,1)S(1)}, f32[4,32,64]{2,1,0:T(8,128)S(1)}) custom-call(bf16[4,512,2048]{2,1,0:T(8,128)(2,1)} %tokens_hbm.1, f32[1,2048]{1,0:T(1,128)} %bitcast.6, bf16[2048,256]{1,0:T(8,128)(2,1)} %wk_hbm.1, bf16[2048,256]{1,0:T(8,128)(2,1)} %wv_hbm.1, bf16[4,4,8,64]{3,2,1,0:T(8,128)(2,1)} %bitcast.4, f32[1,8192]{1,0:T(1,128)} %bitcast.5), custom_call_target="tpu_custom_call" | custom-call | tf_op jit(solution)/shard_map/pallas_call | solution.py:488
  51.5 1.3 %shard_map.78 = (bf16[8192,128]{1,0:T(8,128)(2,1)}, f32[4,32,64]{2,1,0:T(8,128)}) custom-call(bf16[8192,128]{1,0:T(8,128)(2,1)S(1)} %get-tuple-element.6.cache_in, f32[4,32,64]{2,1,0:T(8,128)S(1)} %get-tuple-element.7.read_in), custom_call_target="tpu_custom_call" | custom-call | tf_op jit(solution)/shard_map/pallas_call | solution.py:531
